TPU v7x, 256 devices: a whole 4x4x8 slice. The times are simulated.
256 devices in a mesh: sp: 16 (over y, x), tp: 16 (over z, core).
Axes of the slice: x: 4, y: 4, z: 8, core: 2. Of those that a mesh axis runs over, the one named last changes fastest.
Arguments:
- conv_value: bfloat16 [49152, 2048], P('sp', 'tp'), may hold values from -48 to 48
- conv_gate: bfloat16 [49152, 2048], P('sp', 'tp'), may hold values from -6 to 6
- doc_ids: int32 [49152], P('sp'), may hold values from 0 to 15, never falling along the last dimension, each value on 1 to 9216 neighbouring positions
- conv_kernel: bfloat16 [31, 2048], P(None, 'tp'), may hold values from -1 to 1
- norm_gain_conv: float32 [2048], replicated, may hold values from 0.1 to 1.9
- norm_bias_conv: float32 [2048], replicated, may hold values from -3 to 3
- proj_weight: bfloat16 [2048, 2048], P('tp'), may hold values from -0.125 to 0.125
- residual: bfloat16 [49152, 2048], P(('sp', 'tp')), may hold values from -6 to 6
- norm_gain_moe: float32 [2048], replicated, may hold values from 0.1 to 1.9
- group_router: bfloat16 [2048, 2], replicated, may hold values from -0.125 to 0.125
- expert_router: bfloat16 [2048, 16], replicated, may hold values from -0.125 to 0.125
- routing: int32 [49152, 2], P(('sp', 'tp')), may hold values from 0 to 15, as said below
- expert_gate_w: bfloat16 [16, 2048, 512], P('sp'), may hold values from -0.125 to 0.125
- expert_up_w: bfloat16 [16, 2048, 512], P('sp'), may hold values from -0.125 to 0.125
- expert_down_w: bfloat16 [16, 512, 2048], P('sp'), may hold values from -0.25 to 0.25
Outputs:
- output: bfloat16 [49152, 2048], P(('sp', 'tp'))
Inputs may be any that keep to these rules, and one draw needn't show every extreme that they name: `routing`: both numbers of a row are different experts of one group (expert // 8); within the rows of one device (aligned blocks of 192 rows) every expert is named exactly 24 times.
All inputs are finite; a program needn't handle non-finite values.
Results may differ from a plain program's by a relative error of at most 0.015.
Values may be sent and summed in bfloat16 or wider, within the bound.
No kernel may reach another device: no remote copies, remote signals or barrier semaphores. Data moves between devices by JAX's collectives and lax.ppermute only.
A program may use at most 64 MiB of HBM per device.

v0:
```python
import jax
import jax.numpy as jnp
from jax import lax
from jax.sharding import PartitionSpec as P

epsilon = 1e-06


def shifted(array, axis, by):
    count = lax.axis_size(axis)
    pairs = [(i, i + by) for i in range(count) if 0 <= i + by < count]
    return lax.ppermute(array, axis, pairs)


def project_rows(activated_rows, proj_weight):
    return jnp.dot(
        activated_rows,
        lax.all_gather(proj_weight, "tp", axis=0, tiled=True),
        preferred_element_type=jnp.float32,
    )


def body(
    conv_value,
    conv_gate,
    doc_ids,
    conv_kernel,
    norm_gain_conv,
    norm_bias_conv,
    proj_weight,
    residual,
    norm_gain_moe,
    group_router,
    expert_router,
    routing,
    expert_gate_w,
    expert_up_w,
    expert_down_w,
):
    local_tokens, local_width = conv_value.shape
    kernel_taps = conv_kernel.shape[0]
    rim_width = kernel_taps - 1
    gated_values = (
        conv_value.astype(jnp.float32) * jax.nn.sigmoid(conv_gate.astype(jnp.float32))
    ).astype(jnp.bfloat16)
    rim_values, rim_ids = shifted(
        (gated_values[local_tokens - rim_width :], doc_ids[local_tokens - rim_width :]), "sp", 1
    )
    padded = jnp.concatenate([rim_values, gated_values], axis=0)
    padded_ids = jnp.concatenate([rim_ids, doc_ids], axis=0)
    kernel = conv_kernel.astype(jnp.float32)
    summed = jnp.zeros((local_tokens, local_width), jnp.float32)
    for tap in range(kernel_taps):
        same_doc = padded_ids[tap : tap + local_tokens] == doc_ids
        summed = summed + jnp.where(
            same_doc[:, None],
            padded[tap : tap + local_tokens].astype(jnp.float32) * kernel[tap][None, :],
            jnp.float32(0.0),
        )
    convolved = summed.astype(jnp.bfloat16)
    raw_rows = lax.all_to_all(convolved, "tp", split_axis=0, concat_axis=1, tiled=True)
    raw_values = raw_rows.astype(jnp.float32)
    average = jnp.mean(raw_values, axis=1, keepdims=True)
    centered = raw_values - average
    variance = jnp.mean(centered * centered, axis=1, keepdims=True)
    moved_rows = jax.nn.silu(
        centered * lax.rsqrt(variance + epsilon) * norm_gain_conv + norm_bias_conv
    ).astype(jnp.bfloat16)
    projected = project_rows(moved_rows, proj_weight)
    state_values = residual.astype(jnp.float32) + projected
    hidden_state = state_values.astype(jnp.bfloat16)
    state_values = hidden_state.astype(jnp.float32)
    normed = (
        state_values
        * lax.rsqrt(jnp.mean(state_values * state_values, axis=1, keepdims=True) + epsilon)
        * norm_gain_moe
    ).astype(jnp.bfloat16)
    group_logits = jnp.dot(normed, group_router, preferred_element_type=jnp.float32)
    expert_logits = jnp.dot(normed, expert_router, preferred_element_type=jnp.float32)
    group_total = group_router.shape[1]
    expert_total = expert_router.shape[1]
    per_group = expert_total // group_total
    first_choice = routing[:, 0]
    second_choice = routing[:, 1]
    chosen_group = first_choice // per_group
    group_exp = jnp.exp(group_logits)
    group_match = chosen_group[:, None] == jnp.arange(group_total, dtype=jnp.int32)[None, :]
    group_prob = jnp.sum(jnp.where(group_match, group_exp, jnp.float32(0.0)), axis=1) / jnp.sum(
        group_exp, axis=1
    )
    expert_iota = jnp.arange(expert_total, dtype=jnp.int32)[None, :]
    first_logit = jnp.sum(
        jnp.where(first_choice[:, None] == expert_iota, expert_logits, jnp.float32(0.0)), axis=1
    )
    second_logit = jnp.sum(
        jnp.where(second_choice[:, None] == expert_iota, expert_logits, jnp.float32(0.0)), axis=1
    )
    first_exp = jnp.exp(first_logit)
    second_exp = jnp.exp(second_logit)
    first_weight = group_prob * first_exp / (first_exp + second_exp)
    second_weight = group_prob * second_exp / (first_exp + second_exp)
    row_count = normed.shape[0]
    capacity = 2 * row_count // expert_total
    flat_experts = routing.reshape(-1)
    indicator = (flat_experts[:, None] == expert_iota).astype(jnp.int32)
    before = jnp.cumsum(indicator, axis=0) - indicator
    position = jnp.sum(before * indicator, axis=1)
    destination = flat_experts * capacity + position
    source = (
        jnp.zeros((2 * row_count,), jnp.int32)
        .at[destination]
        .set(jnp.arange(2 * row_count, dtype=jnp.int32) // 2)
    )
    outgoing = normed[source].reshape(expert_total, capacity, normed.shape[1])
    arrived = lax.all_to_all(outgoing, "sp", split_axis=0, concat_axis=0, tiled=True)
    senders, slot_count, features = arrived.shape
    flattened = arrived.reshape(senders * slot_count, features)
    gate_part = jnp.dot(flattened, expert_gate_w[0], preferred_element_type=jnp.float32)
    up_part = jnp.dot(flattened, expert_up_w[0], preferred_element_type=jnp.float32)
    expert_hidden = (jax.nn.silu(gate_part) * up_part).astype(jnp.bfloat16)
    expert_result = jnp.dot(
        expert_hidden, expert_down_w[0], preferred_element_type=jnp.float32
    ).astype(jnp.bfloat16)
    returned = lax.all_to_all(
        expert_result.reshape(senders, slot_count, features),
        "sp",
        split_axis=0,
        concat_axis=0,
        tiled=True,
    )
    picked = (
        returned.reshape(2 * row_count, normed.shape[1])[destination]
        .reshape(row_count, 2, normed.shape[1])
        .astype(jnp.float32)
    )
    mixture = first_weight[:, None] * picked[:, 0] + second_weight[:, None] * picked[:, 1]
    return (state_values + mixture).astype(jnp.bfloat16)


def solution(mesh):
    placed = (
        P("sp", "tp"),
        P("sp", "tp"),
        P("sp"),
        P(None, "tp"),
        P(),
        P(),
        P("tp", None),
        P(("sp", "tp"), None),
        P(),
        P(),
        P(),
        P(("sp", "tp"), None),
        P("sp", None, None),
        P("sp", None, None),
        P("sp", None, None),
    )
    return jax.shard_map(
        body, mesh=mesh, in_specs=placed, out_specs=P(("sp", "tp"), None), check_vma=False
    )
```

profile of v0, /device:TPU:0, one launch (start us, length us, event | category | flops | bytes accessed | tf_op | source)
XLA Modules:
  0.0 186.5 jit_solution(3365401490658242660)
XLA Ops:
  6.5 0.7 all-gather.2.cloned.1.call-update
  7.3 0.8 slice.297
  8.0 1.7 collective-permute-start
  9.7 1.8 multiply_convert_fusion.2
  11.5 3.4 %collective-permute-start.1 = (bf16[30,128]{1,0:T(8,128)(2,1)S(1)}, bf16[30,128]{1,0:T(8,128)(2,1)S(1)}, u32[]{:S(2)}, u32[]{:S(2)}) collective-permute-start(bf16[30,128]{1,0:T(8,128)(2,1)S(1)} %slice.402), channel_id=1, source_target_pairs={{0,16},{16,32},{32,48},{48,64},{64,80},{80,96},{96,112},{112,128},... | collective-permute-start | bytes 23048 | tf_op jit(solution)/shard_map/ppermute | solution.py:12
  15.4 0.8 collective-permute-done.1
  16.3 16.6 %add_convert_fusion = bf16[3072,128]{1,0:T(8,128)(2,1)} fusion(bf16[3072,128]{1,0:T(8,128)(2,1)S(1)} %multiply_convert_fusion.2, bf16[30,128]{1,0:T(8,128)(2,1)S(1)} %collective-permute-done.1, f32[128]{0:T(128)S(1)} %get-tuple-element.14, f32[128]{0:T(128)S(1)} %get-tuple-element.15, f32[128]{0:T(128)S(1)} %get-tuple-element.16, ...), kind=kLoop, calls=%fused_computation.60 | loop fusion | flops 83755008 | bytes 1688576 | tf_op jit(solution)/shard_map/convert_element_type | solution.py:60
  32.9 8.7 %all-to-all-start = ((bf16[16,192,128]{2,1,0:T(8,128)(2,1)}), bf16[16,192,128]{2,1,0:T(8,128)(2,1)S(1)}, u32[]{:S(2)}, u32[]{:S(2)}) async-start(bf16[16,192,128]{2,1,0:T(8,128)(2,1)} %bitcast.147), calls=%async_computation | async-start | bytes 1572864 | tf_op jit(solution)/shard_map/all_to_all | solution.py:61
  42.0 0.9 reduce-window.6
  42.9 0.2 slice_reduce_fusion
  43.3 0.1 mul.522
  43.5 2.9 %scatter_custom_fusion = s32[384]{0:T(512)S(1)} fusion(s32[384]{0:T(512)S(1)} %fusion.132, s32[384]{0:T(512)S(1)} %add_select_fusion, s32[]{:T(128)} %constant.50.clone.1), kind=kCustom, calls=%fused_computation.261 | custom fusion | bytes 1540 | tf_op jit(solution)/shard_map/scatter | solution.py:112
  46.5 25.0 %all-to-all-done = bf16[16,192,128]{2,1,0:T(8,128)(2,1)S(1)} async-done(((bf16[16,192,128]{2,1,0:T(8,128)(2,1)}), bf16[16,192,128]{2,1,0:T(8,128)(2,1)S(1)}, u32[]{:S(2)}, u32[]{:S(2)}) %all-to-all-start) | async-done | bytes 786464 | tf_op jit(solution)/shard_map/all_to_all | solution.py:61
  71.5 0.2 convert_reduce_fusion
  71.7 0.4 fusion.8
  72.1 11.1 %all-gather.2.cloned.1.call-done = bf16[2048,2048]{1,0:T(8,128)(2,1)} async-done(((bf16[128,2048]{1,0:T(8,128)(2,1)}), bf16[2048,2048]{1,0:T(8,128)(2,1)}) %all-gather.2.cloned.1.call-update) | async-done | bytes 8388624 | tf_op jit(solution)/shard_map/all_gather | solution.py:18
  83.2 5.7 %multiply_reduce_fusion = (f32[192]{0:T(256)S(1)}, f32[192,2048]{1,0:T(8,128)S(1)}) fusion(bf16[2048,2048]{1,0:T(8,128)(2,1)} %all-gather.2.cloned.1.call-done, f32[2048]{0:T(1024)S(1)} %copy-done.11, f32[2048]{0:T(1024)S(1)} %copy-done.12, f32[192]{0:T(256)S(1)} %add_rsqrt_fusion.1, f32[192]{0:T(256)S(1)} %broadcast_multiply_fusion.1, ...), kind=kOutput, calls=%fused_computation.58 | convolution fusion | flops 1616903936 | bytes 11553024 | tf_op jit(solution)/shard_map/dot_general | solution.py:16
  88.9 1.1 copy-done.1
  90.0 0.2 multiply_convert_fusion
  90.2 3.1 %gather_fusion = bf16[384,2048]{1,0:T(8,128)(2,1)} fusion(bf16[192,2048]{1,0:T(8,128)(2,1)S(1)} %multiply_convert_fusion, s32[1024]{0:T(1024)S(1)} %pad_clamp_fusion.1), kind=kCustom, calls=%fused_computation | custom fusion | bytes 3147264 | tf_op jit(solution)/shard_map/gather | solution.py:114
  93.3 30.1 %all_to_all.23 = bf16[16,24,2048]{2,1,0:T(8,128)(2,1)S(1)} all-to-all(bf16[16,24,2048]{2,1,0:T(8,128)(2,1)} %bitcast.146), channel_id=1, replica_groups=mesh['sp'=16,'tp'=16] {'sp'}, dimensions={0} | all-to-all | bytes 3145728 | tf_op jit(solution)/shard_map/all_to_all | solution.py:115
  123.5 1.2 copy-done.3
  124.6 1.9 fusion.5
  126.5 5.3 %convolution_convert_fusion = bf16[384,2048]{1,0:T(8,128)(2,1)} fusion(bf16[1,512,2048]{2,1,0:T(8,128)(2,1)S(1)} %copy-done, bf16[384,2048]{1,0:T(8,128)(2,1)} %bitcast.150, bf16[1,2048,512]{2,1,0:T(8,128)(2,1)} %param.28, f32[384,512]{1,0:T(8,128)} %fusion.5), kind=kOutput, calls=%fused_computation.32 | convolution fusion | flops 1612578816 | bytes 8126464 | tf_op jit(solution)/shard_map/dot_general | solution.py:121
  131.8 4.7 %all-to-all-start.2 = ((bf16[16,24,2048]{2,1,0:T(8,128)(2,1)}), bf16[16,24,2048]{2,1,0:T(8,128)(2,1)}, u32[]{:S(2)}, u32[]{:S(2)}) async-start(bf16[16,24,2048]{2,1,0:T(8,128)(2,1)} %bitcast.148), calls=%async_computation.2 | async-start | bytes 3145728 | tf_op jit(solution)/shard_map/all_to_all | solution.py:124
  136.5 0.3 fusion.137
  136.9 0.3 select_reduce_fusion.1
  137.3 22.2 %all-to-all-done.2 = bf16[16,24,2048]{2,1,0:T(8,128)(2,1)} async-done(((bf16[16,24,2048]{2,1,0:T(8,128)(2,1)}), bf16[16,24,2048]{2,1,0:T(8,128)(2,1)}, u32[]{:S(2)}, u32[]{:S(2)}) %all-to-all-start.2) | async-done | bytes 1572896 | tf_op jit(solution)/shard_map/all_to_all | solution.py:124
  159.5 6.7 %gather_fusion.1 = bf16[384,2048]{1,0:T(8,128)(2,1)} fusion(bf16[384,2048]{1,0:T(8,128)(2,1)} %bitcast.43, s32[1024]{0:T(1024)S(1)} %pad_clamp_fusion), kind=kCustom, calls=%fused_computation.1 | custom fusion | bytes 3147264 | tf_op jit(solution)/shard_map/gather | solution.py:132
  166.2 4.7 %reshape.154 = f32[192,2,2048]{2,1,0:T(2,128)} reshape(bf16[384,2048]{1,0:T(8,128)(2,1)} %gather_fusion.1) | data formatting | bytes 4718592 | tf_op jit(solution)/shard_map/convert_element_type | solution.py:134
  170.9 6.2 %fusion.138 = (f32[192,1,2048]{2,1,0:T(1,128)S(1)}, f32[192,1,2048]{2,1,0:T(1,128)S(1)}) fusion(f32[192,2,2048]{2,1,0:T(2,128)} %reshape.154), kind=kLoop, calls=%fused_computation.302 | loop fusion | bytes 6291456 | tf_op jit(solution)/shard_map/slice | solution.py:136
  177.1 2.6 %fusion.15 = bf16[192,2048]{1,0:T(8,128)(2,1)} fusion(f32[192,2048]{1,0:T(8,128)S(1)} %copy-done.2, f32[192,1,2048]{2,1,0:T(1,128)S(1)} %get-tuple-element.12, f32[192,1,2048]{2,1,0:T(1,128)S(1)} %get-tuple-element.11, f32[192]{0:T(256)S(1)} %multiply_divide_fusion, f32[192]{0:T(256)S(1)} %get-tuple-element.9), kind=kLoop, calls=%fused_computation.54 | loop fusion | flops 1966080 | bytes 5506560 | tf_op jit(solution)/shard_map/convert_element_type | solution.py:137
  (53 shorter events, 1.3 us)
Async XLA Ops:
  6.5 119.9 %copy-start = (bf16[1,512,2048]{2,1,0:T(8,128)(2,1)S(1)}, bf16[1,512,2048]{2,1,0:T(8,128)(2,1)}, u32[]{:S(2)}) copy-start(bf16[1,512,2048]{2,1,0:T(8,128)(2,1)} %param.29) | copy-start | bytes 6291460
  6.5 8.5 %copy-start.4 = (s32[3072]{0:T(1024)S(1)}, s32[3072]{0:T(1024)}, u32[]{:S(2)}) copy-start(s32[3072]{0:T(1024)} %param.17) | copy-start | bytes 36868
  6.5 8.4 %copy-start.9 = (bf16[31,128]{1,0:T(8,128)(2,1)S(1)}, bf16[31,128]{1,0:T(8,128)(2,1)}, u32[]{:S(2)}) copy-start(bf16[31,128]{1,0:T(8,128)(2,1)} %param.18) | copy-start | bytes 23812
  6.5 76.6 %all-gather.2.cloned.1.call-start = ((), (), s32[]{:S(2)}) async-start(), calls=%async_computation.3 | async-start | bytes 8912896 | tf_op jit(solution)/shard_map/all_gather | solution.py:18
  8.0 7.0 %collective-permute-start = (s32[30]{0:T(128)S(1)}, s32[30]{0:T(128)S(1)}, u32[]{:S(2)}, u32[]{:S(2)}) collective-permute-start(s32[30]{0:T(128)S(1)} %slice.297), channel_id=1, source_target_pairs={{0,16},{16,32},{32,48},{48,64},{64,80},{80,96},{96,112},{112,128},... | collective-permute-start | bytes 368 | tf_op jit(solution)/shard_map/ppermute | solution.py:12
  11.5 4.8 %collective-permute-start.1 = (bf16[30,128]{1,0:T(8,128)(2,1)S(1)}, bf16[30,128]{1,0:T(8,128)(2,1)S(1)}, u32[]{:S(2)}, u32[]{:S(2)}) collective-permute-start(bf16[30,128]{1,0:T(8,128)(2,1)S(1)} %slice.402), channel_id=1, source_target_pairs={{0,16},{16,32},{32,48},{48,64},{64,80},{80,96},{96,112},{112,128},... | collective-permute-start | bytes 23048 | tf_op jit(solution)/shard_map/ppermute | solution.py:12
  16.3 25.3 %copy-start.6 = (s32[192,2]{0,1:T(2,128)S(1)}, s32[192,2]{0,1:T(2,128)}, u32[]{:S(2)}) copy-start(s32[192,2]{0,1:T(2,128)} %param.26) | copy-start | bytes 4612
  32.9 50.3 %copy-start.11 = (f32[2048]{0:T(1024)S(1)}, f32[2048]{0:T(1024)}, u32[]{:S(2)}) copy-start(f32[2048]{0:T(1024)} %param.20) | copy-start | bytes 24580
  32.9 50.3 %copy-start.12 = (f32[2048]{0:T(1024)S(1)}, f32[2048]{0:T(1024)}, u32[]{:S(2)}) copy-start(f32[2048]{0:T(1024)} %param.19) | copy-start | bytes 24580
  32.9 38.6 %all-to-all-start = ((bf16[16,192,128]{2,1,0:T(8,128)(2,1)}), bf16[16,192,128]{2,1,0:T(8,128)(2,1)S(1)}, u32[]{:S(2)}, u32[]{:S(2)}) async-start(bf16[16,192,128]{2,1,0:T(8,128)(2,1)} %bitcast.147), calls=%async_computation | async-start | bytes 1572864 | tf_op jit(solution)/shard_map/all_to_all | solution.py:61
  72.1 18.0 %copy-start.7 = (f32[2048]{0:T(1024)S(1)}, f32[2048]{0:T(1024)}, u32[]{:S(2)}) copy-start(f32[2048]{0:T(1024)} %param.23) | copy-start | bytes 24580
  88.9 1.1 copy-start.1
  93.3 31.3 %copy-start.10 = (bf16[1,2048,512]{2,1,0:T(8,128)(2,1)S(1)}, bf16[1,2048,512]{2,1,0:T(8,128)(2,1)}, u32[]{:S(2)}) copy-start(bf16[1,2048,512]{2,1,0:T(8,128)(2,1)} %param.27) | copy-start | bytes 6291460
  123.5 1.2 copy-start.3
  131.8 4.7 %copy-start.8 = (bf16[2048,2]{0,1:T(2,128)(2,1)S(1)}, bf16[2048,2]{0,1:T(2,128)(2,1)}, u32[]{:S(2)}) copy-start(bf16[2048,2]{0,1:T(2,128)(2,1)} %param.24) | copy-start | bytes 24580
  131.8 5.1 %copy-start.5 = (bf16[2048,16]{0,1:T(8,128)(2,1)S(1)}, bf16[2048,16]{0,1:T(8,128)(2,1)}, u32[]{:S(2)}) copy-start(bf16[2048,16]{0,1:T(8,128)(2,1)} %param.25) | copy-start | bytes 196612
  131.8 27.7 %all-to-all-start.2 = ((bf16[16,24,2048]{2,1,0:T(8,128)(2,1)}), bf16[16,24,2048]{2,1,0:T(8,128)(2,1)}, u32[]{:S(2)}, u32[]{:S(2)}) async-start(bf16[16,24,2048]{2,1,0:T(8,128)(2,1)} %bitcast.148), calls=%async_computation.2 | async-start | bytes 3145728 | tf_op jit(solution)/shard_map/all_to_all | solution.py:124
  170.9 6.2 %copy-start.2 = (f32[192,2048]{1,0:T(8,128)S(1)}, f32[192,2048]{1,0:T(8,128)}, u32[]{:S(2)}) copy-start(f32[192,2048]{1,0:T(8,128)} %copy-done.1) | copy-start | bytes 4718596
Sparse Core Ops, SparseCore 0:
  9.2 73.9 all-gather.1
where the time goes:
time: 187 us
  waiting for transfers between devices  59.9 us (32%)
  blocking collectives  30.1 us (16%)
  local copies, waits for them, and re-layouts  27.6 us (15%)
  other arithmetic  23.2 us (12%)
  starting transfers between devices  18.5 us (10%)
  between operations  13.7 us (7%)
  matrix products  13.5 us (7%)
    all_to_all x1, blocking collectives, body(): lax.all_to_all(outgoing, 'sp', split_axis=0, concat_axis=0, tiled=True)  30.1 us
    all_to_all x1, waiting for transfers between devices, body(): lax.all_to_all(convolved, 'tp', split_axis=0, concat_axis=1, tiled=True)  25 us
    all_to_all x1, waiting for transfers between devices, body(): lax.all_to_all(expert_result.reshape(senders, slot_count, features), 'sp'...  22.2 us
    convert_element_type x1, other arithmetic, body(): convolved = summed.astype(jnp.bfloat16)  16.6 us
    all_gather x1, waiting for transfers between devices, project_rows(): lax.all_gather(proj_weight, 'tp', axis=0, tiled=True)  11.1 us
    all_to_all x1, starting transfers between devices, body(): lax.all_to_all(convolved, 'tp', split_axis=0, concat_axis=1, tiled=True)  8.7 us
    gather x1, local copies, waits for them, and re-layouts, body(): returned.reshape(2 * row_count, normed.shape[1])[destination]  6.68 us
    slice x1, local copies, waits for them, and re-layouts, body(): picked[:, 0]  6.18 us
  transfers between devices with their start and end apart: 5, of which 4 were waited for; matrix products, arithmetic and copies ran while one was open for 14% of the time, Pallas kernels for 0%

commit v1 on v0

--- a/solution.py
+++ b/solution.py
@@ -4,6 +4,11 @@
 from jax.sharding import PartitionSpec as P
 
 epsilon = 1e-06
+
+
+def gather_over(x, mesh_axis, d):
+    outgoing = jnp.stack([x] * lax.axis_size(mesh_axis))
+    return jnp.concatenate(lax.all_to_all(outgoing, mesh_axis, 0, 0), axis=d)
 
 
 def shifted(array, axis, by):
@@ -14,9 +19,7 @@
 
 def project_rows(activated_rows, proj_weight):
     return jnp.dot(
-        activated_rows,
-        lax.all_gather(proj_weight, "tp", axis=0, tiled=True),
-        preferred_element_type=jnp.float32,
+        activated_rows, gather_over(proj_weight, "tp", 0), preferred_element_type=jnp.float32
     )
 
 

time: 187 us -> 347 us (1.86)
  waiting for transfers between devices: 59.9 us -> 201 us
  blocking collectives: 30.1 us -> 60.9 us
  between operations: 13.7 us -> 0.34 us
  starting transfers between devices: 18.5 us -> 14.5 us
  local copies, waits for them, and re-layouts: 27.6 us -> 31.2 us
    all_to_all x1, waiting for transfers between devices: 25 us -> 179 us  [gather_over(): return jnp.concatenate(lax.all_to_all(outgoing, mesh_axis, 0, 0), axis=d)]
    all_to_all x0 -> x1, blocking collectives: none -> 30.7 us  [body(): lax.all_to_all(convolved, 'tp', split_axis=0, concat_axis=1, tiled=True)]
    all_gather x1 -> x0, waiting for transfers between devices: 11.1 us -> none  [project_rows(): lax.all_gather(proj_weight, 'tp', axis=0, tiled=True)]
    another operation x0 -> x1, local copies, waits for them, and re-layouts: none -> 4.28 us  [gather_over(): outgoing = jnp.stack([x] * lax.axis_size(mesh_axis))]
    all_to_all x1, starting transfers between devices: 8.7 us -> 4.87 us  [gather_over(): return jnp.concatenate(lax.all_to_all(outgoing, mesh_axis, 0, 0), axis=d)]
  transfers between devices with their start and end apart: 5 -> 4, of which waited for: 4 -> 3; matrix products, arithmetic and copies ran while one was open for 14% -> 2% of each run, Pallas kernels for 0% -> 0%
where the time goes in v1:
time: 347 us; the launch traced here: 345 us
  waiting for transfers between devices  201 us (58%)
  blocking collectives  60.9 us (18%)
  local copies, waits for them, and re-layouts  31.2 us (9%)
  other arithmetic  22.6 us (7%)
  starting transfers between devices  14.5 us (4%)
  matrix products  13.5 us (4%)
    all_to_all x1, waiting for transfers between devices, gather_over(): return jnp.concatenate(lax.all_to_all(outgoing, mesh_axis, 0, 0), axis=d)  179 us
    all_to_all x1, blocking collectives, body(): lax.all_to_all(convolved, 'tp', split_axis=0, concat_axis=1, tiled=True)  30.7 us
    all_to_all x1, blocking collectives, body(): lax.all_to_all(outgoing, 'sp', split_axis=0, concat_axis=0, tiled=True)  30.1 us
    all_to_all x1, waiting for transfers between devices, body(): lax.all_to_all(expert_result.reshape(senders, slot_count, features), 'sp'...  21.7 us
    convert_element_type x1, other arithmetic, body(): convolved = summed.astype(jnp.bfloat16)  15.9 us
  transfers between devices with their start and end apart: 4, of which 3 were waited for; matrix products, arithmetic and copies ran while one was open for 2% of the time, Pallas kernels for 0%

profile of v1, /device:TPU:0, one launch (start us, length us, event | category | flops | bytes accessed | tf_op | source)
XLA Modules:
  0.0 344.5 jit_solution(3846514867258101514)
XLA Ops:
  0.0 1.9 multiply_convert_fusion.1
  2.0 1.7 collective-permute-start.1
  3.7 3.4 collective-permute-start
  7.2 1.2 collective-permute-done
  8.9 15.9 %add_convert_fusion = bf16[3072,128]{1,0:T(8,128)(2,1)S(1)} fusion(bf16[3072,128]{1,0:T(8,128)(2,1)S(1)} %multiply_convert_fusion.1, bf16[30,128]{1,0:T(8,128)(2,1)S(1)} %collective-permute-done.1, f32[128]{0:T(128)S(1)} %get-tuple-element.14, f32[128]{0:T(128)S(1)} %get-tuple-element.15, f32[128]{0:T(128)S(1)} %get-tuple-element.16, ...), kind=kLoop, calls=%fused_computation.65 | loop fusion | flops 83755008 | bytes 1688576 | tf_op jit(solution)/shard_map/convert_element_type | solution.py:63
  24.8 30.7 %all_to_all.28 = bf16[16,192,128]{2,1,0:T(8,128)(2,1)S(1)} all-to-all(bf16[16,192,128]{2,1,0:T(8,128)(2,1)S(1)} %bitcast.158), channel_id=1, replica_groups=mesh['sp'=16,'tp'=16] {'tp'}, dimensions={0} | all-to-all | bytes 1572864 | tf_op jit(solution)/shard_map/all_to_all | solution.py:64
  55.5 4.3 %stack.2 = bf16[16,128,2048]{2,1,0:T(8,128)(2,1)} broadcast(bf16[128,2048]{1,0:T(8,128)(2,1)S(1)} %copy-done.4), dimensions={1,2} | broadcast | bytes 8912896 | tf_op jit(solution)/shard_map/stack | solution.py:10
  59.8 4.9 %all-to-all-start.1 = ((bf16[16,128,2048]{2,1,0:T(8,128)(2,1)}), bf16[16,128,2048]{2,1,0:T(8,128)(2,1)}, u32[]{:S(2)}, u32[]{:S(2)}) async-start(bf16[16,128,2048]{2,1,0:T(8,128)(2,1)} %stack.2), calls=%async_computation.1 | async-start | bytes 16777216 | tf_op jit(solution)/shard_map/all_to_all | solution.py:11
  64.8 0.1 eq.202
  65.2 0.1 mul.533
  65.4 0.9 reduce-window.6
  66.3 0.2 slice_reduce_fusion
  66.6 2.9 scatter_custom_fusion
  69.6 0.2 convert_reduce_fusion
  69.8 0.4 fusion.10
  70.1 178.6 %all-to-all-done.1 = bf16[16,128,2048]{2,1,0:T(8,128)(2,1)} async-done(((bf16[16,128,2048]{2,1,0:T(8,128)(2,1)}), bf16[16,128,2048]{2,1,0:T(8,128)(2,1)}, u32[]{:S(2)}, u32[]{:S(2)}) %all-to-all-start.1) | async-done | bytes 8388640 | tf_op jit(solution)/shard_map/all_to_all | solution.py:11
  248.7 5.7 %multiply_reduce_fusion = (f32[192]{0:T(256)S(1)}, f32[192,2048]{1,0:T(8,128)S(1)}) fusion(bf16[16,128,2048]{2,1,0:T(8,128)(2,1)} %all-to-all-done.1, bf16[16,192,128]{2,1,0:T(8,128)(2,1)S(1)} %all_to_all.28, f32[16,128]{1,0:T(8,128)S(1)} %bitcast.166, f32[16,128]{1,0:T(8,128)S(1)} %bitcast.167, f32[192]{0:T(256)S(1)} %add_rsqrt_fusion.1, ...), kind=kOutput, calls=%fused_computation.64 | convolution fusion | flops 1616903936 | bytes 11553024 | tf_op jit(solution)/shard_map/dot_general | solution.py:21
  254.5 1.1 copy-done.1
  255.6 0.2 multiply_convert_fusion
  255.8 3.1 gather_fusion
  258.9 30.1 %all_to_all.29 = bf16[16,24,2048]{2,1,0:T(8,128)(2,1)S(1)} all-to-all(bf16[16,24,2048]{2,1,0:T(8,128)(2,1)} %bitcast.157), channel_id=1, replica_groups=mesh['sp'=16,'tp'=16] {'sp'}, dimensions={0} | all-to-all | bytes 3145728 | tf_op jit(solution)/shard_map/all_to_all | solution.py:118
  289.1 1.2 copy-done.3
  290.2 1.9 fusion.6
  292.1 5.3 %convolution_convert_fusion = bf16[384,2048]{1,0:T(8,128)(2,1)} fusion(bf16[1,512,2048]{2,1,0:T(8,128)(2,1)S(1)} %copy-done, bf16[384,2048]{1,0:T(8,128)(2,1)} %bitcast.161, bf16[1,2048,512]{2,1,0:T(8,128)(2,1)} %param.28, f32[384,512]{1,0:T(8,128)} %fusion.6), kind=kOutput, calls=%fused_computation.32 | convolution fusion | flops 1612578816 | bytes 8126464 | tf_op jit(solution)/shard_map/dot_general | solution.py:124
  297.4 4.5 %all-to-all-start.3 = ((bf16[16,24,2048]{2,1,0:T(8,128)(2,1)}), bf16[16,24,2048]{2,1,0:T(8,128)(2,1)}, u32[]{:S(2)}, u32[]{:S(2)}) async-start(bf16[16,24,2048]{2,1,0:T(8,128)(2,1)} %bitcast.159), calls=%async_computation.3 | async-start | bytes 3145728 | tf_op jit(solution)/shard_map/all_to_all | solution.py:127
  302.0 0.3 fusion.146
  302.3 0.3 select_reduce_fusion.1
  302.7 21.7 %all-to-all-done.3 = bf16[16,24,2048]{2,1,0:T(8,128)(2,1)} async-done(((bf16[16,24,2048]{2,1,0:T(8,128)(2,1)}), bf16[16,24,2048]{2,1,0:T(8,128)(2,1)}, u32[]{:S(2)}, u32[]{:S(2)}) %all-to-all-start.3) | async-done | bytes 1572896 | tf_op jit(solution)/shard_map/all_to_all | solution.py:127
  324.4 6.7 %gather_fusion.1 = bf16[384,2048]{1,0:T(8,128)(2,1)} fusion(bf16[384,2048]{1,0:T(8,128)(2,1)} %bitcast.46, s32[1024]{0:T(1024)S(1)} %pad_clamp_fusion), kind=kCustom, calls=%fused_computation.1 | custom fusion | bytes 3147264 | tf_op jit(solution)/shard_map/gather | solution.py:135
  331.1 4.7 %reshape.175 = f32[192,2,2048]{2,1,0:T(2,128)} reshape(bf16[384,2048]{1,0:T(8,128)(2,1)} %gather_fusion.1) | data formatting | bytes 4718592 | tf_op jit(solution)/shard_map/convert_element_type | solution.py:137
  335.8 6.2 %fusion.147 = (f32[192,1,2048]{2,1,0:T(1,128)S(1)}, f32[192,1,2048]{2,1,0:T(1,128)S(1)}) fusion(f32[192,2,2048]{2,1,0:T(2,128)} %reshape.175), kind=kLoop, calls=%fused_computation.307 | loop fusion | bytes 6291456 | tf_op jit(solution)/shard_map/slice | solution.py:139
  342.0 2.6 fusion.23
  (54 shorter events, 1.2 us)
Async XLA Ops:
  0.0 292.1 %copy-start = (bf16[1,512,2048]{2,1,0:T(8,128)(2,1)S(1)}, bf16[1,512,2048]{2,1,0:T(8,128)(2,1)}, u32[]{:S(2)}) copy-start(bf16[1,512,2048]{2,1,0:T(8,128)(2,1)} %param.29) | copy-start | bytes 6291460
  0.0 3.7 %copy-start.5 = (s32[3072]{0:T(1024)S(1)}, s32[3072]{0:T(1024)}, u32[]{:S(2)}) copy-start(s32[3072]{0:T(1024)} %param.17) | copy-start | bytes 36868
  0.0 7.1 %copy-start.10 = (bf16[31,128]{1,0:T(8,128)(2,1)S(1)}, bf16[31,128]{1,0:T(8,128)(2,1)}, u32[]{:S(2)}) copy-start(bf16[31,128]{1,0:T(8,128)(2,1)} %param.18) | copy-start | bytes 23812
  2.0 6.9 %collective-permute-start.1 = (bf16[30,128]{1,0:T(8,128)(2,1)S(1)}, bf16[30,128]{1,0:T(8,128)(2,1)S(1)}, u32[]{:S(2)}, u32[]{:S(2)}) collective-permute-start(bf16[30,128]{1,0:T(8,128)(2,1)S(1)} %slice.402), channel_id=1, source_target_pairs={{0,16},{16,32},{32,48},{48,64},{64,80},{80,96},{96,112},{112,128},... | collective-permute-start | bytes 23048 | tf_op jit(solution)/shard_map/ppermute | solution.py:17
  3.7 4.7 %collective-permute-start = (s32[30]{0:T(128)S(1)}, s32[30]{0:T(128)S(1)}, u32[]{:S(2)}, u32[]{:S(2)}) collective-permute-start(s32[30]{0:T(128)S(1)} %slice.297), channel_id=1, source_target_pairs={{0,16},{16,32},{32,48},{48,64},{64,80},{80,96},{96,112},{112,128},... | collective-permute-start | bytes 368 | tf_op jit(solution)/shard_map/ppermute | solution.py:17
  8.9 46.6 %copy-start.4 = (bf16[128,2048]{1,0:T(8,128)(2,1)S(1)}, bf16[128,2048]{1,0:T(8,128)(2,1)}, u32[]{:S(2)}) copy-start(bf16[128,2048]{1,0:T(8,128)(2,1)} %param.21) | copy-start | bytes 1572868
  59.8 4.9 %copy-start.7 = (s32[192,2]{0,1:T(2,128)S(1)}, s32[192,2]{0,1:T(2,128)}, u32[]{:S(2)}) copy-start(s32[192,2]{0,1:T(2,128)} %param.26) | copy-start | bytes 4612
  59.8 189.0 %all-to-all-start.1 = ((bf16[16,128,2048]{2,1,0:T(8,128)(2,1)}), bf16[16,128,2048]{2,1,0:T(8,128)(2,1)}, u32[]{:S(2)}, u32[]{:S(2)}) async-start(bf16[16,128,2048]{2,1,0:T(8,128)(2,1)} %stack.2), calls=%async_computation.1 | async-start | bytes 16777216 | tf_op jit(solution)/shard_map/all_to_all | solution.py:11
  64.7 184.1 %copy-start.12 = (f32[2048]{0:T(1024)S(1)}, f32[2048]{0:T(1024)}, u32[]{:S(2)}) copy-start(f32[2048]{0:T(1024)} %param.20) | copy-start | bytes 24580
  64.7 184.1 %copy-start.13 = (f32[2048]{0:T(1024)S(1)}, f32[2048]{0:T(1024)}, u32[]{:S(2)}) copy-start(f32[2048]{0:T(1024)} %param.19) | copy-start | bytes 24580
  248.7 6.9 %copy-start.8 = (f32[2048]{0:T(1024)S(1)}, f32[2048]{0:T(1024)}, u32[]{:S(2)}) copy-start(f32[2048]{0:T(1024)} %param.23) | copy-start | bytes 24580
  254.5 1.1 copy-start.1
  258.9 31.3 %copy-start.11 = (bf16[1,2048,512]{2,1,0:T(8,128)(2,1)S(1)}, bf16[1,2048,512]{2,1,0:T(8,128)(2,1)}, u32[]{:S(2)}) copy-start(bf16[1,2048,512]{2,1,0:T(8,128)(2,1)} %param.27) | copy-start | bytes 6291460
  289.1 1.2 copy-start.3
  297.4 4.6 %copy-start.9 = (bf16[2048,2]{0,1:T(2,128)(2,1)S(1)}, bf16[2048,2]{0,1:T(2,128)(2,1)}, u32[]{:S(2)}) copy-start(bf16[2048,2]{0,1:T(2,128)(2,1)} %param.24) | copy-start | bytes 24580
  297.4 4.9 %copy-start.6 = (bf16[2048,16]{0,1:T(8,128)(2,1)S(1)}, bf16[2048,16]{0,1:T(8,128)(2,1)}, u32[]{:S(2)}) copy-start(bf16[2048,16]{0,1:T(8,128)(2,1)} %param.25) | copy-start | bytes 196612
  297.4 27.0 %all-to-all-start.3 = ((bf16[16,24,2048]{2,1,0:T(8,128)(2,1)}), bf16[16,24,2048]{2,1,0:T(8,128)(2,1)}, u32[]{:S(2)}, u32[]{:S(2)}) async-start(bf16[16,24,2048]{2,1,0:T(8,128)(2,1)} %bitcast.159), calls=%async_computation.3 | async-start | bytes 3145728 | tf_op jit(solution)/shard_map/all_to_all | solution.py:127
  335.8 6.2 %copy-start.2 = (f32[192,2048]{1,0:T(8,128)S(1)}, f32[192,2048]{1,0:T(8,128)}, u32[]{:S(2)}) copy-start(f32[192,2048]{1,0:T(8,128)} %copy-done.1) | copy-start | bytes 4718596
